TPU v7x, 32 devices: a whole 2x2x4 slice. The times are simulated.
32 devices in a mesh: sp: 4 (over z), dp: 8 (over y, x, core).
Axes of the slice: x: 2, y: 2, z: 4, core: 2. Of those that a mesh axis runs over, the one named last changes fastest.
Arguments:
- tokens: bfloat16 [8, 512, 2048], P('dp', 'sp'), may hold values from -6 to 6
- receptance_weight: bfloat16 [2048, 1024], P('dp'), may hold values from -0.125 to 0.125
- key_projection_weight: bfloat16 [2048, 1024], P('dp'), may hold values from -0.125 to 0.125
- value_projection_weight: bfloat16 [2048, 1024], P('dp'), may hold values from -0.125 to 0.125
- decay_down_weight: bfloat16 [2048, 256], P('dp'), may hold values from -0.125 to 0.125
- decay_up_weight: bfloat16 [2, 128, 1024], replicated, may hold values from -0.71875 to 0.71875
- decay_floor_level: float32 [2, 1024], replicated, may hold values from -10 to -2.25
- correction_rate_logit: float32 [2, 1024], P(None, 'sp'), may hold values from -4 to 4
- diagonal_address_factor: float32 [2, 1024], P(None, 'sp'), may hold values from -1 to 1
- head_norm_gain: float32 [1024], P('sp'), may hold values from 0.1 to 1.9
Outputs:
- mixed: bfloat16 [8, 512, 1024], P('dp', 'sp')
All inputs are finite; a program needn't handle non-finite values.
Results may differ from a plain program's by a relative error of at most 0.0056.
The roundings to bfloat16 on the way count: a program that leaves them out, or rounds other values in their place, can miss the bound.
Values may be sent and summed in bfloat16 or wider, within the bound.
A program may use at most 128 MiB of HBM per device.

v0:
```python
import functools
import math

import jax
import jax.numpy as jnp
from jax import lax
from jax.experimental import pallas as pl
from jax.experimental.pallas import tpu as pltpu
from jax.sharding import PartitionSpec as P

HEAD = 64
SPAN = 64
BF = jnp.bfloat16
F32 = jnp.float32
NT = (((1,), (1,)), ((), ()))
TN = (((0,), (0,)), ((), ()))


def mm(a, b):
    return jnp.dot(a, b, preferred_element_type=F32)


def split(x):
    hi = x.astype(BF)
    return hi, (x - hi.astype(F32)).astype(BF)


def iota(shape, axis):
    return lax.broadcasted_iota(jnp.int32, shape, axis)


def core_kernel(
    tok_ref, w_ref, up_ref, floor_ref, rate_ref, diag_ref, gain_ref, out_ref,
    eq_s, wp_s, qe_s, kend_s, cv_s, own_s, decay_s, diag_s, t_s, b_s, state_s, y_s,
    arrivals=(),
):
    length, chans = out_ref.shape
    heads = chans // HEAD
    rank = up_ref.shape[1]
    rows = min(256, length)
    blocks = length // SPAN

    def head_ones():
        return (iota((chans, chans), 0) // HEAD == iota((chans, chans), 1) // HEAD).astype(BF)

    def head_sum(x, ones):
        hi, lo = split(x)
        return mm(hi, ones) + mm(lo, ones)

    def at_block(block):
        return pl.ds(pl.multiple_of(block * SPAN, SPAN), SPAN)

    def project(ready):
        tile = SPAN * len(ready)

        def put(ref, x, *lead):
            for s, block in enumerate(ready):
                ref[(*lead, at_block(block), slice(None))] = x[s * SPAN : (s + 1) * SPAN]

        source = jnp.concatenate([tok_ref[at_block(block), :] for block in ready], axis=0)
        pr = mm(source, w_ref[:, :chans]).astype(BF).astype(F32)
        pk = mm(source, w_ref[:, chans : 2 * chans]).astype(BF).astype(F32)
        pv = mm(source, w_ref[:, 2 * chans : 3 * chans]).astype(BF).astype(F32)
        lowered = jnp.tanh(mm(source, w_ref[:, 3 * chans :])).astype(BF)
        ones = head_ones()
        norm2 = head_sum(pk * pk, ones) + 1.0
        inv = lax.rsqrt(norm2)
        scale = norm2 * inv
        normed = pk * inv
        put(cv_s, scale * pv)
        rates = jax.nn.sigmoid(rate_ref[...])
        both = jnp.sum(rates * diag_ref[...], axis=0, keepdims=True)
        put(own_s, head_sum(pr * pk * both, ones) * pv)
        ri = iota((tile, tile), 0)
        ci = iota((tile, tile), 1)
        same = ri // SPAN == ci // SPAN
        whole = same.astype(BF)
        for d in range(2):
            pre = (
                mm(lowered[:, d * rank : (d + 1) * rank], up_ref[d]) + floor_ref[d : d + 1, :]
            ).astype(BF).astype(F32)
            fall = -math.exp(-0.5) * jax.nn.sigmoid(pre)
            tri = jnp.logical_and(same, (ci <= ri) if d == 0 else (ci >= ri)).astype(BF)
            hi, lo = split(fall)
            inclusive = mm(tri, hi) + mm(tri, lo)
            final = mm(whole, hi) + mm(whole, lo)
            half = 0.5 * final
            grow = jnp.exp(inclusive - half)
            shrink = jnp.exp(half - inclusive)
            g = jnp.exp(half)
            e = -normed * (grow * jnp.exp(-fall))
            q = pr * grow
            w = normed * rates[d : d + 1, :] * shrink
            put(wp_s, w.astype(BF), d)
            put(kend_s, (w * g).astype(BF), d)
            eb, qb = e.astype(BF), q.astype(BF)
            eg, qg = (e * g).astype(BF), (q * g).astype(BF)
            g2 = g * g
            put(diag_s, head_sum(pr * normed * rates[d : d + 1, :], ones), d)
            for s, block in enumerate(ready):
                cut = slice(s * SPAN, (s + 1) * SPAN)
                base = pl.multiple_of(block * 2 * SPAN, 2 * SPAN)
                eq_s[d, pl.ds(base, SPAN), :] = eb[cut]
                eq_s[d, pl.ds(base + SPAN, SPAN), :] = qb[cut]
                qe_s[d, pl.ds(base, SPAN), :] = eg[cut]
                qe_s[d, pl.ds(base + SPAN, SPAN), :] = qg[cut]
                decay_s[d, pl.ds(pl.multiple_of(block * 8, 8), 8), :] = g2[
                    s * SPAN : s * SPAN + 8
                ]

    def spread(x, mask):
        x = x.astype(BF)
        if heads > 1:
            x = jnp.concatenate([x] * heads, axis=0)
        return x * mask

    def invert(ready):
        mask = head_ones()
        ti = iota((SPAN, chans), 0)
        ji = iota((SPAN, chans), 1) % HEAD
        eye = (ti == ji).astype(F32)
        work = []
        for block in ready:
            for d in range(2):
                two = pl.ds(pl.multiple_of(block * 2 * SPAN, 2 * SPAN), 2 * SPAN)
                at = pl.ds(pl.multiple_of(block * SPAN, SPAN), SPAN)
                ab = lax.dot_general(
                    eq_s[d, two, :], spread(wp_s[d, at, :], mask), NT, preferred_element_type=F32
                )
                strict = (ti > ji) if d == 0 else (ti < ji)
                b_s[d, at, :] = jnp.where(strict, ab[SPAN:], 0.0).astype(BF)
                work.append((d, at, jnp.where(strict, ab[:SPAN], 0.0)))
        near = ti // 4 == ji // 4
        full = [a for _, _, a in work]
        base = [jnp.where(near, a, 0.0) for a in full]
        square = [mm(a.astype(BF), spread(a, mask)) for a in base]
        inverse = [eye + a for a in base]
        inverse = [t + mm(t.astype(BF), spread(a2, mask)) for t, a2 in zip(inverse, square)]
        size = 4
        while size < SPAN:
            far = jnp.logical_and(ti // (2 * size) == ji // (2 * size), ti // size != ji // size)
            first = [
                mm(t.astype(BF), spread(jnp.where(far, a, 0.0), mask))
                for t, a in zip(inverse, full)
            ]
            inverse = [t + mm(f.astype(BF), spread(t, mask)) for t, f in zip(inverse, first)]
            size *= 2
        for (d, at, _), t in zip(work, inverse):
            t_s[d, at, :] = (t - eye).astype(BF)

    for settle, ready in arrivals:
        settle()
        project(ready)
        invert(ready)

    state_s[...] = jnp.zeros_like(state_s)

    @pl.loop(0, blocks)
    def _(step):
        mask = head_ones()
        for d in range(2):
            block = step if d == 0 else blocks - 1 - step
            two = pl.ds(pl.multiple_of(block * 2 * SPAN, 2 * SPAN), 2 * SPAN)
            at = pl.ds(pl.multiple_of(block * SPAN, SPAN), SPAN)
            state = state_s[d]
            read = lax.dot_general(
                qe_s[d, two, :], state.astype(BF), NT, preferred_element_type=F32
            )
            x = cv_s[at, :] + read[:SPAN]
            exact = x + mm(t_s[d, at, :], spread(x, mask))
            a = exact.astype(BF)
            y_s[d, at, :] = read[SPAN:] + mm(b_s[d, at, :], spread(a, mask)) + diag_s[d, at, :] * exact
            decay = decay_s[d, pl.ds(pl.multiple_of(block * 8, 8), 8), :][:1]
            put = lax.dot_general(a, kend_s[d, at, :], TN, preferred_element_type=F32)
            state_s[d] = state * decay + put * mask.astype(F32)

    @pl.loop(0, length // rows)
    def _(step):
        at = pl.ds(pl.multiple_of(step * rows, rows), rows)
        ones = head_ones()
        total = own_s[at, :]
        for d in range(2):
            y = y_s[d, at, :]
            centred = y - head_sum(y, ones) * (1.0 / HEAD)
            variance = head_sum(centred * centred, ones) * (1.0 / HEAD)
            total = total + centred * lax.rsqrt(variance + 0.00064) * gain_ref[...]
        out_ref[at, :] = total.astype(BF)


MESH = pl.DeviceIdType.MESH


def whole_kernel(
    sp, dp, tok_ref, w_ref, up_ref, floor_ref, rate_ref, diag_ref, gain_ref, out_ref,
    tok_all, w_all, out_all, slots,
    ring_out, ring_in, far_out, far_in, pass_out, pass_in, back_out, back_in, *scratch,
):
    rows = tok_ref.shape[0]
    half_rows = rows // 2
    depth = w_ref.shape[0]
    chans = out_all.shape[1]
    chips = dp // 2
    z = lax.axis_index("sp")
    me = lax.axis_index("dp")
    chip = me // 2
    core = me % 2
    partner = chip * 2 + 1 - core

    def peer(k):
        return lax.rem(chip + k, chips) * 2 + core

    def z_peer(k):
        return lax.rem(z + k, sp)

    barrier = pltpu.get_barrier_semaphore()
    for target in [(z, partner)] + [(z, peer(k)) for k in range(1, chips)] + [
        (z_peer(k), me) for k in range(1, sp)
    ]:
        pl.semaphore_signal(barrier, inc=1, device_id=target, device_id_type=MESH)
    pl.semaphore_wait(barrier, chips + sp - 1)

    def remote(src, dst, out_sem, in_sem, target):
        copy = pltpu.make_async_remote_copy(
            src_ref=src, dst_ref=dst, send_sem=out_sem, recv_sem=in_sem,
            device_id=target, device_id_type=MESH,
        )
        copy.start()
        return copy

    def w_at(device):
        return pl.ds(pl.multiple_of(device * depth, depth), depth)

    def ring_step(s):
        copies = []
        for way in range(2):
            owner = z_peer(sp - s) if way == 0 else z_peer(s)
            at = pl.ds(
                pl.multiple_of(owner * rows + way * half_rows, half_rows), half_rows
            )
            first = tok_ref.at[pl.ds(way * half_rows, half_rows), :]
            copies.append(
                remote(
                    first if s == 0 else tok_all.at[at, :], tok_all.at[at, :],
                    ring_out.at[way, s], ring_in.at[way, s],
                    (z_peer(1) if way == 0 else z_peer(sp - 1), me),
                )
            )
        return copies

    ring = [ring_step(0)] if sp > 1 else []
    far = [
        remote(w_ref, w_all.at[w_at(me), :], far_out.at[k], far_in.at[k], (z, peer(k)))
        for k in range(1, chips)
    ]
    passed = [remote(w_ref, w_all.at[w_at(me), :], pass_out.at[0], pass_in.at[0], (z, partner))]
    w_all[w_at(me), :] = w_ref[...]
    tok_all[pl.ds(pl.multiple_of(z * rows, rows), rows), :] = tok_ref[...]
    for s in range(max(sp, chips) - 1):
        if s < sp - 2:
            for copy in ring[s]:
                copy.wait_recv()
            ring.append(ring_step(s + 1))
        if s < chips - 1:
            far[s].wait_recv()
            block = w_at(peer(chips - 1 - s))
            passed.append(
                remote(
                    w_all.at[block, :], w_all.at[block, :],
                    pass_out.at[s + 1], pass_in.at[s + 1], (z, partner),
                )
            )
    for copy in passed:
        copy.wait_recv()

    def last_ring():
        for copy in ring[-1]:
            copy.wait_recv()

    per = rows // SPAN
    arrivals = [(lambda: None, [z * per + b for b in range(per)])]
    for s in range(sp - 1):
        before, after = z_peer(sp - 1 - s), z_peer(s + 1)
        ready = [before * per + b for b in range(per // 2)]
        ready += [after * per + b for b in range(per // 2, per)]
        arrivals.append((last_ring if s == sp - 2 else lambda: None, ready))

    core_kernel(
        tok_all, w_all, up_ref, floor_ref, rate_ref, diag_ref, gain_ref, out_all, *scratch,
        arrivals=arrivals,
    )
    for copy in far + passed + [c for pair in ring for c in pair]:
        copy.wait_send()

    def out_at(owner):
        return pl.ds(pl.multiple_of(owner * rows, rows), rows)

    back = [
        remote(
            out_all.at[out_at(z_peer(k)), :], slots.at[z], back_out.at[k], back_in.at[k],
            (z_peer(k), me),
        )
        for k in range(1, sp)
    ]
    slots[z] = out_all[out_at(z), :]
    for copy in back:
        copy.wait()
    for s in range(sp):
        out_ref[:, s * chans : (s + 1) * chans] = slots[s]


def whole_call(sp, dp, rows, depth, chans, width):
    vm = pltpu.VMEM
    dma = pltpu.SemaphoreType.DMA
    length = rows * sp
    both = lambda n, dt: vm((2, n, chans), dt)
    return pl.pallas_call(
        functools.partial(whole_kernel, sp, dp),
        out_shape=jax.ShapeDtypeStruct((rows, chans * sp), BF),
        in_specs=[pl.BlockSpec(memory_space=vm)] * 7,
        out_specs=pl.BlockSpec(memory_space=vm),
        scratch_shapes=[
            vm((length, depth), BF), vm((depth, width), BF), vm((length, chans), BF),
            vm((sp, rows, chans), BF),
            dma((2, sp)), dma((2, sp)), dma((dp,)), dma((dp,)), dma((dp,)), dma((dp,)),
            dma((sp,)), dma((sp,)),
            both(2 * length, BF), both(length, BF), both(2 * length, BF), both(length, BF),
            vm((length, chans), F32), vm((length, chans), F32),
            both(length // SPAN * 8, F32), both(length, F32), both(length, BF), both(length, BF),
            vm((2, chans, chans), F32), both(length, F32),
        ],
        compiler_params=pltpu.CompilerParams(
            vmem_limit_bytes=58 * 1024 * 1024, collective_id=0, has_side_effects=True
        ),
        name="whole",
    )


def per_device(
    sp, dp,
    tokens, receptance_weight, key_projection_weight, value_projection_weight,
    decay_down_weight, decay_up_weight, decay_floor_level, correction_rate_logit,
    diagonal_address_factor, head_norm_gain,
):
    rows, depth = tokens.shape[1:]
    channels = receptance_weight.shape[1]
    chans = channels // sp
    start = lax.axis_index("sp") * chans

    def mine(x):
        return lax.dynamic_slice_in_dim(x, start, chans, axis=x.ndim - 1)

    packed = jnp.concatenate(
        [mine(receptance_weight), mine(key_projection_weight), mine(value_projection_weight),
         decay_down_weight], axis=1)
    mixed = whole_call(sp, dp, rows, depth, chans, packed.shape[1])(
        tokens[0], packed, mine(decay_up_weight), mine(decay_floor_level),
        correction_rate_logit, diagonal_address_factor, head_norm_gain[None, :])
    return mixed[None]


def solution(mesh):
    in_specs = (
        P("dp", "sp", None), P("dp", None), P("dp", None), P("dp", None), P("dp", None),
        P(), P(), P(None, "sp"), P(None, "sp"), P("sp"),
    )
    return jax.shard_map(
        functools.partial(per_device, mesh.shape["sp"], mesh.shape["dp"]), mesh=mesh, in_specs=in_specs,
        out_specs=P("dp", "sp", None), check_vma=False,
    )
```

profile of v0, /device:TPU:0, one launch (start us, length us, event | category | flops | bytes accessed | tf_op | source)
XLA Modules:
  0.0 71.2 jit_solution(15353320635220030655)
XLA Ops:
  0.0 0.0 copy-start
  0.0 1.0 %constant_dynamic-slice_fusion.2 = (bf16[256,256]{1,0:T(8,128)(2,1)S(1)}, bf16[256,256]{1,0:T(8,128)(2,1)S(1)}) fusion(bf16[256,1024]{1,0:T(8,128)(2,1)} %param.13, s32[]{:T(128)S(6)} %select_n.2, bf16[256,1024]{1,0:T(8,128)(2,1)} %param.12), kind=kLoop, calls=%fused_computation.3 | loop fusion | bytes 524292 | tf_op jit(solution)/shard_map/dynamic_slice | solution.py:350
  1.1 0.1 copy-done
  1.2 0.0 copy-start.1
  1.2 0.9 %copy-done.1 = bf16[256,256]{1,0:T(8,128)(2,1)S(1)} copy-done((bf16[256,256]{1,0:T(8,128)(2,1)S(1)}, bf16[256,256]{1,0:T(8,128)(2,1)}, u32[]{:S(2)}) %copy-start.1) | copy-done | bytes 131096
  2.1 0.9 %pad_maximum_fusion.w_ref = bf16[256,1024]{1,0:T(8,128)(2,1)} fusion(bf16[256,256]{1,0:T(8,128)(2,1)S(1)} %copy-done.1, bf16[256,256]{1,0:T(8,128)(2,1)S(1)} %get-tuple-element.5, bf16[256,256]{1,0:T(8,128)(2,1)S(1)} %get-tuple-element.6, bf16[256,256]{1,0:T(8,128)(2,1)S(1)} %constant_dynamic-slice_fusion.4), kind=kLoop, calls=%fused_computation | loop fusion | flops 2097152 | bytes 1048576 | tf_op jit(solution)/shard_map/concatenate | solution.py:352
  2.9 1.6 %constant_dynamic-slice_fusion.1.up_ref = bf16[2,128,256]{2,1,0:T(8,128)(2,1)} fusion(bf16[2,128,1024]{2,1,0:T(8,128)(2,1)} %param.15, s32[]{:T(128)S(6)} %select_n.2), kind=kLoop, calls=%fused_computation.2 | loop fusion | bytes 262148 | tf_op jit(solution)/shard_map/dynamic_slice | solution.py:350
  4.5 1.3 %constant_dynamic-slice_fusion.floor_ref = f32[2,256]{1,0:T(2,128)} fusion(f32[2,1024]{1,0:T(2,128)} %param.16, s32[]{:T(128)S(6)} %select_n.2), kind=kLoop, calls=%fused_computation.1 | loop fusion | bytes 4100 | tf_op jit(solution)/shard_map/dynamic_slice | solution.py:350
  5.8 63.8 %whole.1 = bf16[128,1024]{1,0:T(8,128)(2,1)} custom-call(bf16[128,2048]{1,0:T(8,128)(2,1)} %bitcast.4, bf16[256,1024]{1,0:T(8,128)(2,1)} %pad_maximum_fusion.w_ref, bf16[2,128,256]{2,1,0:T(8,128)(2,1)} %constant_dynamic-slice_fusion.1.up_ref, f32[2,256]{1,0:T(2,128)} %constant_dynamic-slice_fusion.floor_ref, f32[2,256]{1,0:T(2,128)} %rate_ref.1, ...), custom_call_target="tpu_custom_call" | custom-call | tf_op jit(solution)/shard_map/whole/pallas_call | solution.py:355
  69.6 1.7 %copy.12 = bf16[1,128,1024]{2,1,0:T(8,128)(2,1)} copy(bf16[1,128,1024]{2,1,0:T(8,128)(2,1)} %bitcast.3) | data formatting | bytes 524288
  (1 shorter events, 0.0 us)
Async XLA Ops:
  0.0 1.2 %copy-start = (bf16[256,1024]{1,0:T(8,128)(2,1)S(1)}, bf16[256,1024]{1,0:T(8,128)(2,1)}, u32[]{:S(2)}) copy-start(bf16[256,1024]{1,0:T(8,128)(2,1)} %param.11) | copy-start | bytes 1572868
  1.2 0.9 %copy-start.1 = (bf16[256,256]{1,0:T(8,128)(2,1)S(1)}, bf16[256,256]{1,0:T(8,128)(2,1)}, u32[]{:S(2)}) copy-start(bf16[256,256]{1,0:T(8,128)(2,1)} %param.14) | copy-start | bytes 393220
where the time goes:
time: 71.5 us; the launch traced here: 71.2 us
  Pallas kernels  63.8 us (89%)
  local copies, waits for them, and re-layouts  6.56 us (9%)
  other arithmetic  0.86 us (1%)
    pallas_call x1, Pallas kernels, per_device(): whole_call(sp, dp, rows, depth, chans, packed.shape[1])  63.8 us
    dynamic_slice x4, local copies, waits for them, and re-layouts, mine(): return lax.dynamic_slice_in_dim(x, start, chans, axis=x.ndim - 1)  3.89 us
    unnamed x5, local copies, waits for them, and re-layouts  2.68 us

commit v1 on v0

--- a/solution.py
+++ b/solution.py
@@ -1,13 +1,9 @@
-import functools
-import math
-
-import jax
-import jax.numpy as jnp
+import functools, math
+import jax, jax.numpy as jnp
 from jax import lax
 from jax.experimental import pallas as pl
 from jax.experimental.pallas import tpu as pltpu
 from jax.sharding import PartitionSpec as P
-
 HEAD = 64
 SPAN = 64
 BF = jnp.bfloat16
@@ -20,6 +16,10 @@
     return jnp.dot(a, b, preferred_element_type=F32)
 
 
+def dot(a, b, dims):
+    return lax.dot_general(a, b, dims, preferred_element_type=F32)
+
+
 def split(x):
     hi = x.astype(BF)
     return hi, (x - hi.astype(F32)).astype(BF)
@@ -27,6 +27,202 @@
 
 def iota(shape, axis):
     return lax.broadcasted_iota(jnp.int32, shape, axis)
+
+
+def head_ones(chans):
+    return (iota((chans, chans), 0) // HEAD == iota((chans, chans), 1) // HEAD).astype(BF)
+
+
+def head_sum(x, ones):
+    hi, lo = split(x)
+    return mm(hi, ones) + mm(lo, ones)
+
+
+def spread(x, mask):
+    x = x.astype(BF)
+    heads = mask.shape[0] // HEAD
+    if heads > 1:
+        x = jnp.concatenate([x] * heads, axis=0)
+    return x * mask
+
+
+def at_row(start, size):
+    return pl.ds(pl.multiple_of(start, size), size)
+
+
+class Core:
+    def __init__(self, tok, wk, wd, wv, wr, up, floor, rate, diag, gain, out, scratch):
+        self.tok, self.wk, self.wd, self.wv, self.wr = tok, wk, wd, wv, wr
+        self.up, self.floor, self.rate, self.diag, self.gain, self.out = up, floor, rate, diag, gain, out
+        (self.pk_s, self.pv_s, self.inv_s, self.grow_s, self.g_s, self.wp_s, self.kend_s,
+         self.t_s, self.teg_s, self.step_s, self.tcv_s, self.put_s, self.state_s) = scratch
+        self.length, self.chans = out.shape
+        self.heads = self.chans // HEAD
+        self.rank = up.shape[1]
+        self.blocks = self.length // SPAN
+        self.half = self.length // 2
+
+    def unit(self, block):
+        return at_row(block * SPAN, SPAN)
+
+    def keys(self, start):
+        chans, rank, tile = self.chans, self.rank, self.half
+        many = tile // SPAN
+        ones = head_ones(chans)
+        at = at_row(start, tile)
+        source = self.tok[at, :]
+        pk = mm(source, self.wk[...]).astype(BF)
+        self.pk_s[at, :] = pk
+        pk = pk.astype(F32)
+        lowered = jnp.tanh(mm(source, self.wd[...])).astype(BF)
+        inv = lax.rsqrt(head_sum(pk * pk, ones) + 1.0)
+        self.inv_s[at, :] = inv
+        normed = pk * inv
+        rates = jax.nn.sigmoid(self.rate[...])
+        ri = iota((tile, tile), 0)
+        ci = iota((tile, tile), 1)
+        same = ri // SPAN == ci // SPAN
+        first = start // SPAN
+        units = []
+        for d in range(2):
+            pre = (
+                mm(lowered[:, d * rank : (d + 1) * rank], self.up[d]) + self.floor[d : d + 1, :]
+            ).astype(BF).astype(F32)
+            fall = -math.exp(-0.5) * jax.nn.sigmoid(pre)
+            tri = jnp.logical_and(same, (ci <= ri) if d == 0 else (ci >= ri)).astype(BF)
+            hi, lo = split(fall)
+            inclusive = mm(tri, hi) + mm(tri, lo)
+            rated = normed * rates[d : d + 1, :]
+            for s in range(many):
+                cut = slice(s * SPAN, (s + 1) * SPAN)
+                inside = inclusive[cut]
+                end = inside[SPAN - 1 :] if d == 0 else inside[:1]
+                mid = 0.5 * end
+                inside = inside - mid
+                g = jnp.exp(mid)
+                grow = jnp.exp(inside)
+                e = -normed[cut] * jnp.exp(inside - fall[cut])
+                w = rated[cut] * jnp.exp(-inside)
+                here = self.unit(first + s)
+                self.grow_s[d, here, :] = grow
+                self.g_s[d, pl.ds(pl.multiple_of((first + s) * 8, 8), 8), :] = jnp.broadcast_to(g, (8, chans))
+                w = w.astype(BF)
+                kend = (w.astype(F32) * g).astype(BF)
+                self.wp_s[d, here, :] = w
+                self.kend_s[d, here, :] = kend
+                units.append((d, first + s, e.astype(BF), w, kend, (e * g).astype(BF)))
+        return units
+
+    def strict(self, d):
+        ti = iota((SPAN, self.chans), 0)
+        ji = iota((SPAN, self.chans), 1) % HEAD
+        return (ti > ji) if d == 0 else (ti < ji)
+
+    def invert(self, units):
+        chans = self.chans
+        mask = head_ones(chans)
+        ti = iota((SPAN, chans), 0)
+        ji = iota((SPAN, chans), 1) % HEAD
+        eye = (ti == ji).astype(F32)
+        full = [
+            jnp.where(self.strict(d), dot(e, spread(w, mask), NT), 0.0) for d, _, e, w, _, _ in units
+        ]
+        near = ti // 4 == ji // 4
+        base = [jnp.where(near, a, 0.0) for a in full]
+        square = [mm(a.astype(BF), spread(a, mask)) for a in base]
+        inverse = [eye + a for a in base]
+        inverse = [t + mm(t.astype(BF), spread(a2, mask)) for t, a2 in zip(inverse, square)]
+        size = 4
+        while size < SPAN:
+            far = jnp.logical_and(ti // (2 * size) == ji // (2 * size), ti // size != ji // size)
+            first = [
+                mm(t.astype(BF), spread(jnp.where(far, a, 0.0), mask))
+                for t, a in zip(inverse, full)
+            ]
+            inverse = [t + mm(f.astype(BF), spread(t, mask)) for t, f in zip(inverse, first)]
+            size *= 2
+        for (d, block, _, _, kend, eg), t in zip(units, inverse):
+            here = self.unit(block)
+            t = (t - eye).astype(BF)
+            self.t_s[d, here, :] = t
+            teg = (eg.astype(F32) + mm(t, spread(eg, mask))).astype(BF)
+            self.teg_s[d, here, :] = teg
+            self.step_s[d, at_row(block * chans, chans), :] = dot(teg, kend, TN).astype(BF) * mask
+
+    def values(self):
+        chans = self.chans
+        mask = head_ones(chans)
+        pv = mm(self.tok[...], self.wv[...]).astype(BF)
+        self.pv_s[...] = pv
+        cv = pv.astype(F32) / self.inv_s[...]
+        for block in range(self.blocks):
+            cut = slice(block * SPAN, (block + 1) * SPAN)
+            x = cv[cut]
+            for d in range(2):
+                tcv = x + mm(self.t_s[d, cut, :], spread(x, mask))
+                self.tcv_s[d, cut, :] = tcv
+                put = dot(tcv.astype(BF), self.kend_s[d, cut, :], TN) * mask.astype(F32)
+                self.put_s[d, cut, :] = sum(put[h * HEAD : (h + 1) * HEAD] for h in range(self.heads))
+
+    def scan(self):
+        states = [jnp.zeros((HEAD, self.chans), F32) for _ in range(2)]
+        for step in range(self.blocks):
+            for d in range(2):
+                block = step if d == 0 else self.blocks - 1 - step
+                cut = slice(block * SPAN, (block + 1) * SPAN)
+                state = states[d]
+                low = state.astype(BF)
+                self.state_s[d, cut, :] = low
+                if step < self.blocks - 1:
+                    g = self.g_s[d, block * 8 : block * 8 + 1, :]
+                    step_w = self.step_s[d, block * self.chans : (block + 1) * self.chans, :]
+                    states[d] = state * (g * g) + mm(low, step_w) + self.put_s[d, cut, :]
+
+    def outputs(self, start, tile):
+        chans = self.chans
+        mask = head_ones(chans)
+        at = at_row(start, tile)
+        first = start // SPAN
+        pr = mm(self.tok[at, :], self.wr[...]).astype(BF).astype(F32)
+        pp = pr * self.pk_s[at, :].astype(F32)
+        rates = jax.nn.sigmoid(self.rate[...])
+        both = jnp.sum(rates * self.diag[...], axis=0, keepdims=True)
+        total = head_sum(pp * both, mask) * self.pv_s[at, :].astype(F32)
+        inv = self.inv_s[at, :]
+        for d in range(2):
+            ys = []
+            diag = head_sum(pp * rates[d : d + 1, :], mask) * inv
+            for s in range(tile // SPAN):
+                cut = slice(s * SPAN, (s + 1) * SPAN)
+                here = self.unit(first + s)
+                g = self.g_s[d, pl.ds(pl.multiple_of((first + s) * 8, 8), 8), :][:1]
+                q = pr[cut] * self.grow_s[d, here, :]
+                qb = q.astype(BF)
+                qg = (q * g).astype(BF)
+                b = jnp.where(self.strict(d), dot(qb, spread(self.wp_s[d, here, :], mask), NT), 0.0)
+                read = dot(
+                    jnp.concatenate([self.teg_s[d, here, :], qg], axis=0),
+                    spread(self.state_s[d, here, :], mask), NT,
+                )
+                exact = self.tcv_s[d, here, :] + read[:SPAN]
+                ys.append(read[SPAN:] + mm(b.astype(BF), spread(exact, mask)) + diag[cut] * exact)
+            y = jnp.concatenate(ys, axis=0)
+            centred = y - head_sum(y, mask) * (1.0 / HEAD)
+            variance = head_sum(centred * centred, mask) * (1.0 / HEAD)
+            total = total + centred * lax.rsqrt(variance + 0.00064) * self.gain[...]
+        self.out[at, :] = total.astype(BF)
+
+
+def core_scratch(length, chans):
+    vm = pltpu.VMEM
+    both = lambda n, dt: vm((2, n, chans), dt)
+    blocks = length // SPAN
+    return [
+        vm((length, chans), BF), vm((length, chans), BF), vm((length, chans), F32),
+        both(length, F32), both(blocks * 8, F32), both(length, BF), both(length, BF),
+        both(length, BF), both(length, BF), both(blocks * chans, BF), both(length, F32),
+        both(length, F32), both(length, BF),
+    ]
 
 
 def core_kernel(
@@ -335,15 +531,402 @@
     )
 
 
+def halves_kernel(
+    sp, side, other, tok_ref, wr_ref, wk_ref, wv_ref, wd_ref, up_ref, floor_ref, rate_ref, diag_ref, gain_ref,
+    out_ref, tok_all, wk_all, wv_all, wr_all, wd_all, up_s, floor_s, rate_s, diag_s, gain_s, out_all,
+    w_in, w_out, relay_out, d_in, d_pass, t_in, t_pass, t_out, t_fwd, p_in, p_out, o_in, o_out, here, *scratch,
+):
+    rows = tok_ref.shape[0]
+    depth = wk_ref.shape[0]
+    chans = wk_all.shape[1]
+    half = sp // 2
+    part = rows // 2
+    z = lax.axis_index("sp")
+    me = lax.axis_index("dp")
+    core = me % 2
+    chip = me // 2
+    cy, cx = chip // side, chip % side
+    h = z // half
+    j = z % half
+    u = jnp.where(h == 1, j, half - 1 - j)
+    slot = u * 2 + core
+    partner = chip * 2 + 1 - core
+
+    def layer(hh, uu):
+        return half - 1 - uu + hh * (2 * uu + 1)
+
+    def x_peer(k):
+        return cy * side + lax.rem(cx + k, side)
+
+    def y_peer(k):
+        return lax.rem(cy + k, other) * side + cx
+
+    x_peers = [x_peer(k) for k in range(1, side)]
+    y_peers = [y_peer(k) for k in range(1, other)]
+
+    def local(src, dst, n):
+        copy = pltpu.make_async_copy(src, dst, here.at[n])
+        copy.start()
+        return copy
+
+    def cols(who):
+        return pl.ds(pl.multiple_of(who * chans, chans), chans)
+
+    mine = at_row(me * depth, depth)
+    own = [
+        local(wd_ref, wd_all.at[mine, :], 0),
+        local(wk_ref.at[:, cols(slot)], wk_all.at[mine, :], 1),
+        local(up_ref.at[:, :, cols(slot)], up_s, 2),
+        local(floor_ref.at[:, cols(slot)], floor_s, 3),
+        local(wv_ref.at[:, cols(slot)], wv_all.at[mine, :], 4),
+        local(wr_ref.at[:, cols(slot)], wr_all.at[mine, :], 5),
+    ]
+
+    @pl.when(core == h)
+    def _():
+        local(tok_ref, tok_all.at[at_row(z * rows, rows), :], 6)
+
+    barrier = pltpu.get_barrier_semaphore()
+    greet = [(z, p * 2 + k) for p in x_peers + y_peers for k in range(2)]
+    greet += [(lax.rem(z + n, sp), chip * 2 + k) for n in range(1, sp) for k in range(2)]
+    greet.append((z, partner))
+    for target in greet:
+        pl.semaphore_signal(barrier, inc=1, device_id=target, device_id_type=MESH)
+    pl.semaphore_wait(barrier, len(greet))
+
+    def remote(src, dst, out_sem, in_sem, target):
+        return pltpu.make_async_remote_copy(
+            src_ref=src, dst_ref=dst, send_sem=out_sem, recv_sem=in_sem,
+            device_id=target, device_id_type=MESH,
+        )
+
+    def go(copy):
+        copy.start()
+        return copy
+
+    sent = []
+    pieces = [(wk_ref, wk_all), (wv_ref, wv_all), (wr_ref, wr_all)]
+
+    def direct(n):
+        src, dst = pieces[n]
+        for i, p in enumerate(x_peers + y_peers):
+            for k in range(2):
+                sent.append(go(remote(
+                    src.at[:, cols(u * 2 + k)], dst.at[mine, :],
+                    w_out.at[n, i * 2 + k], w_in.at[n, me], (z, p * 2 + k),
+                )))
+        last = 2 * len(x_peers + y_peers)
+        sent.append(go(remote(
+            src.at[:, cols(u * 2 + 1 - core)], dst.at[mine, :],
+            w_out.at[n, last], w_in.at[n, me], (z, partner),
+        )))
+
+    def arrived(sem, dst, block):
+        remote(dst.at[block, :], dst.at[block, :], sem, sem, (z, partner)).wait_recv()
+
+    def w_rows(p, c):
+        return at_row((p * 2 + c) * depth, depth)
+
+    def relay(n):
+        dst = pieces[n][1]
+        count = 0
+        for c, froms, tos in ((0, x_peers, y_peers), (1, y_peers, x_peers)):
+            for p in froms:
+                block = w_rows(p, c)
+                arrived(w_in.at[n, p * 2 + c], dst, block)
+                for q in tos:
+                    sent.append(go(remote(
+                        dst.at[block, :], dst.at[block, :],
+                        relay_out.at[n, count], w_in.at[n, p * 2 + c], (z, q * 2 + core),
+                    )))
+                    count += 1
+
+    def finish(n):
+        dst = pieces[n][1]
+        for c, others in ((1, x_peers), (0, y_peers)):
+            for p in others:
+                arrived(w_in.at[n, p * 2 + c], dst, w_rows(p, c))
+        for ky in range(1, other):
+            for kx in range(1, side):
+                p = lax.rem(cy + ky, other) * side + lax.rem(cx + kx, side)
+                for c in range(2):
+                    arrived(w_in.at[n, p * 2 + c], dst, w_rows(p, c))
+        arrived(w_in.at[n, partner], dst, w_rows(chip, 1 - core))
+
+    def decay_direct():
+        for i, p in enumerate(x_peers + y_peers):
+            sent.append(go(remote(
+                wd_ref, wd_all.at[mine, :], w_out.at[3, i], d_in.at[me], (z, p * 2 + core))))
+        sent.append(go(remote(
+            wd_ref, wd_all.at[mine, :], w_out.at[3, len(x_peers + y_peers)], d_in.at[me], (z, partner))))
+
+    def decay_pass(p, n):
+        block = w_rows(p, core)
+        sent.append(go(remote(
+            wd_all.at[block, :], wd_all.at[block, :], d_pass.at[n], d_in.at[p * 2 + core], (z, partner))))
+
+    late = []
+
+    def decay_relay():
+        for c, froms, tos in ((0, x_peers, y_peers), (1, y_peers, x_peers)):
+            @pl.when(core == c)
+            def _():
+                count = 0
+                for p in froms:
+                    block = w_rows(p, c)
+                    arrived(d_in.at[p * 2 + c], wd_all, block)
+                    for q in tos:
+                        go(remote(
+                            wd_all.at[block, :], wd_all.at[block, :],
+                            relay_out.at[3, count], d_in.at[p * 2 + c], (z, q * 2 + c)))
+                        count += 1
+                for p in tos:
+                    arrived(d_in.at[p * 2 + c], wd_all, w_rows(p, c))
+
+            def close(c=c, froms=froms, tos=tos):
+                @pl.when(core == c)
+                def _():
+                    count = 0
+                    for p in froms:
+                        block = w_rows(p, c)
+                        for q in tos:
+                            remote(
+                                wd_all.at[block, :], wd_all.at[block, :],
+                                relay_out.at[3, count], d_in.at[p * 2 + c], (z, q * 2 + c)).wait_send()
+                            count += 1
+
+            late.append(close)
+        for n, p in enumerate(x_peers + y_peers):
+            decay_pass(p, n)
+
+    def decay_finish():
+        n = len(x_peers + y_peers)
+        corners = [
+            lax.rem(cy + ky, other) * side + lax.rem(cx + kx, side)
+            for ky in range(1, other) for kx in range(1, side)
+        ]
+        for p in corners:
+            arrived(d_in.at[p * 2 + core], wd_all, w_rows(p, core))
+            decay_pass(p, n)
+            n += 1
+        arrived(d_in.at[partner], wd_all, w_rows(chip, 1 - core))
+        for p in x_peers + y_peers + corners:
+            arrived(d_in.at[p * 2 + 1 - core], wd_all, w_rows(p, 1 - core))
+
+    def t_rows(s, i):
+        return at_row(s * rows + i * part, part)
+
+    def block_sends(act):
+        def both_parts(target_layer, first):
+            for i in range(2):
+                act(remote(
+                    tok_ref.at[pl.ds(i * part, part), :], tok_all.at[t_rows(z, i), :],
+                    t_out.at[first + i], t_in.at[z], (target_layer, chip * 2 + i)))
+
+        @pl.when(core != h)
+        def _():
+            both_parts(layer(core, 0), 0)
+
+        @pl.when(jnp.logical_and(core == h, u + 1 < half))
+        def _():
+            both_parts(layer(h, u + 1), 0)
+
+        @pl.when(jnp.logical_and(core == h, u > 0))
+        def _():
+            both_parts(layer(h, u - 1), 2)
+
+        @pl.when(core == h)
+        def _():
+            act(remote(
+                tok_ref, tok_all.at[at_row(z * rows, rows), :], t_out.at[4], t_pass.at[z], (z, partner)))
+
+    def forward(s, outward, inward, n, act):
+        block = t_rows(s, core)
+        for cond, step in ((outward, 1), (inward, -1)):
+            if cond is not None:
+                @pl.when(cond)
+                def _():
+                    act(remote(
+                        tok_all.at[block, :], tok_all.at[block, :], t_fwd.at[n], t_in.at[s],
+                        (layer(h, u + step), me)))
+        act(remote(
+            tok_all.at[block, :], tok_all.at[block, :], t_fwd.at[sp + n], t_pass.at[s], (z, partner)))
+
+    near = [lax.rem(u + k, half) for k in range(1, half)]
+    sources = [
+        (layer(h, v), jnp.logical_and(u > v, u + 1 < half), jnp.logical_and(u < v, u > 0)) for v in near
+    ]
+    sources += [(layer(1 - h, v), u + 1 < half, None) for v in range(half)]
+
+    def take_tokens(n):
+        s, outward, inward = sources[n]
+        arrived(t_in.at[s], tok_all, t_rows(s, core))
+        forward(s, outward, inward, n, go)
+
+    def own_tokens():
+        block = at_row(z * rows, rows)
+
+        @pl.when(core == h)
+        def _():
+            pltpu.make_async_copy(tok_ref, tok_all.at[block, :], here.at[6]).wait()
+
+        @pl.when(core != h)
+        def _():
+            arrived(t_pass.at[z], tok_all, block)
+
+    def passed_tokens(n):
+        s = sources[n][0]
+        arrived(t_pass.at[s], tok_all, t_rows(s, 1 - core))
+
+    goal = (layer(core, z // 2), chip * 2 + z % 2)
+    stay = jnp.logical_and(goal[0] == z, z % 2 == core)
+    smalls = [(rate_ref, rate_s), (diag_ref, diag_s), (gain_ref, gain_s)]
+
+    @pl.when(jnp.logical_not(stay))
+    def _():
+        for n, (src, dst) in enumerate(smalls):
+            go(remote(src, dst, p_out.at[n], p_in.at[n], goal))
+
+    @pl.when(stay)
+    def _():
+        for n, (src, dst) in enumerate(smalls):
+            pltpu.make_async_copy(src, dst, p_in.at[n]).start()
+
+    decay_direct()
+    block_sends(go)
+    direct(0)
+    decay_relay()
+    relay(0)
+    direct(1)
+    direct(2)
+    for n in range(len(sources)):
+        take_tokens(n)
+    decay_finish()
+    finish(0)
+    for copy in own[:4]:
+        copy.wait()
+    own_tokens()
+    for n in range(half - 1):
+        passed_tokens(n)
+
+    @pl.when(jnp.logical_not(stay))
+    def _():
+        for n, (src, dst) in enumerate(smalls):
+            remote(src, dst, p_out.at[n], p_in.at[n], goal).wait_send()
+    for n, (src, dst) in enumerate(smalls):
+        remote(dst, dst, p_in.at[n], p_in.at[n], (z, partner)).wait_recv()
+
+    work = Core(
+        tok_all, wk_all, wd_all, wv_all, wr_all, up_s, floor_s, rate_s, diag_s, gain_s, out_all, scratch)
+    near_rows = h * half * rows
+    far_rows = (1 - h) * half * rows
+    units = work.keys(near_rows)
+    relay(1)
+    work.invert(units)
+    for n in range(half - 1, len(sources)):
+        passed_tokens(n)
+    units = work.keys(far_rows)
+    relay(2)
+    work.invert(units)
+    finish(1)
+    own[4].wait()
+    work.values()
+    work.scan()
+    finish(2)
+    own[5].wait()
+
+    def give(s, n, act):
+        block = at_row(s * rows, rows)
+        act(remote(
+            out_all.at[block, :], out_ref.at[:, cols(slot)], o_out.at[n], o_in.at[slot],
+            (s, chip * 2 + h)))
+
+    work.outputs(far_rows, half * rows)
+    for v in range(half):
+        give(layer(1 - h, v), v, go)
+    work.outputs(near_rows, half * rows)
+    for n in range(half - 1):
+        give(sources[n][0], half + n, go)
+
+    @pl.when(core != h)
+    def _():
+        give(z, sp - 1, go)
+
+    @pl.when(core == h)
+    def _():
+        out_ref[:, cols(slot)] = out_all[at_row(z * rows, rows), :]
+
+    def stop(copy):
+        copy.wait_send()
+
+    block_sends(stop)
+    for n, (s, outward, inward) in enumerate(sources):
+        forward(s, outward, inward, n, stop)
+    for copy in sent:
+        copy.wait_send()
+    for close in late:
+        close()
+    for v in range(half):
+        give(layer(1 - h, v), v, stop)
+    for n in range(half - 1):
+        give(sources[n][0], half + n, stop)
+
+    @pl.when(core != h)
+    def _():
+        give(z, sp - 1, stop)
+
+    for g in range(sp):
+        @pl.when(jnp.logical_not(jnp.logical_and(core == h, slot == g)))
+        def _():
+            remote(
+                out_all.at[pl.ds(0, rows), :], out_ref.at[:, g * chans : (g + 1) * chans],
+                o_in.at[g], o_in.at[g], (z, partner)).wait_recv()
+
+
+def halves_call(sp, dp, side, rows, width, depth, chans, rank):
+    vm = pltpu.VMEM
+    dma = pltpu.SemaphoreType.DMA
+    chips = dp // 2
+    other = chips // side
+    peers = side + other - 2
+    corners = (side - 1) * (other - 1)
+    length = rows * sp
+    return pl.pallas_call(
+        functools.partial(halves_kernel, sp, side, other),
+        out_shape=jax.ShapeDtypeStruct((rows, chans * sp), BF),
+        in_specs=[pl.BlockSpec(memory_space=pl.ANY)] * 10,
+        out_specs=pl.BlockSpec(memory_space=vm),
+        scratch_shapes=[
+            vm((length, width), BF), vm((width, chans), BF), vm((width, chans), BF), vm((width, chans), BF),
+            vm((width, 2 * rank), BF), vm((2, rank, chans), BF), vm((2, chans), F32), vm((2, chans), F32),
+            vm((2, chans), F32), vm((1, chans), F32), vm((length, chans), BF),
+            dma((3, dp)), dma((4, 2 * peers + 1)), dma((4, 2 * corners)), dma((dp,)), dma((peers + corners,)),
+            dma((sp,)), dma((sp,)), dma((5,)), dma((2 * sp,)), dma((3,)), dma((3,)), dma((sp,)), dma((sp,)),
+            dma((7,)),
+        ] + core_scratch(length, chans),
+        compiler_params=pltpu.CompilerParams(
+            vmem_limit_bytes=58 * 1024 * 1024, collective_id=0, has_side_effects=True
+        ),
+        name="halves",
+    )
+
+
 def per_device(
     sp, dp,
     tokens, receptance_weight, key_projection_weight, value_projection_weight,
     decay_down_weight, decay_up_weight, decay_floor_level, correction_rate_logit,
     diagonal_address_factor, head_norm_gain,
 ):
-    rows, depth = tokens.shape[1:]
-    channels = receptance_weight.shape[1]
+    rows, width = tokens.shape[1:]
+    depth, channels = receptance_weight.shape
     chans = channels // sp
+    side = math.isqrt(dp // 2)
+    gain = head_norm_gain[None, :]
+    if chans % 128 == 0 and sp % 2 == 0 and dp == 2 * side * side and rows % (2 * SPAN) == 0:
+        mixed = halves_call(sp, dp, side, rows, width, depth, chans, decay_up_weight.shape[1])(
+            tokens[0], receptance_weight, key_projection_weight, value_projection_weight, decay_down_weight,
+            decay_up_weight, decay_floor_level, correction_rate_logit, diagonal_address_factor, gain)
+        return mixed[None]
     start = lax.axis_index("sp") * chans
 
     def mine(x):
@@ -352,9 +935,9 @@
     packed = jnp.concatenate(
         [mine(receptance_weight), mine(key_projection_weight), mine(value_projection_weight),
          decay_down_weight], axis=1)
-    mixed = whole_call(sp, dp, rows, depth, chans, packed.shape[1])(
+    mixed = whole_call(sp, dp, rows, width, chans, packed.shape[1])(
         tokens[0], packed, mine(decay_up_weight), mine(decay_floor_level),
-        correction_rate_logit, diagonal_address_factor, head_norm_gain[None, :])
+        correction_rate_logit, diagonal_address_factor, gain)
     return mixed[None]
 
 

time: 71.5 us -> 55.6 us (0.78)
  Pallas kernels: 63.8 us -> 53.8 us
  local copies, waits for them, and re-layouts: 6.56 us -> 1.67 us
  other arithmetic: 0.86 us -> 0 us
    pallas_call x1, Pallas kernels: 63.8 us -> 53.8 us  [per_device(): halves_call(sp, dp, side, rows, width, depth, chans, decay_up_weight.shap...]
    dynamic_slice x4 -> x0, local copies, waits for them, and re-layouts: 3.89 us -> none  [mine(): return lax.dynamic_slice_in_dim(x, start, chans, axis=x.ndim - 1)]
    unnamed x5 -> x1, local copies, waits for them, and re-layouts: 2.68 us -> 1.67 us
    concatenate x1 -> x0, other arithmetic: 0.86 us -> none  [per_device(): jnp.concatenate([mine(receptance_weight), mine(key_projection_weight), mi...]
where the time goes in v1:
time: 55.6 us; the launch traced here: 55.5 us
  Pallas kernels  53.8 us (97%)
  local copies, waits for them, and re-layouts  1.67 us (3%)
    pallas_call x1, Pallas kernels, per_device(): halves_call(sp, dp, side, rows, width, depth, chans, decay_up_weight.shap...  53.8 us
    unnamed x1, local copies, waits for them, and re-layouts  1.67 us

profile of v1, /device:TPU:0, one launch (start us, length us, event | category | flops | bytes accessed | tf_op | source)
XLA Modules:
  0.0 55.5 jit_solution(8621021781203516446)
XLA Ops:
  0.0 53.8 %halves.1 = bf16[128,1024]{1,0:T(8,128)(2,1)} custom-call(bf16[128,2048]{1,0:T(8,128)(2,1)} %bitcast.4, bf16[256,1024]{1,0:T(8,128)(2,1)} %wr_ref.1, bf16[256,1024]{1,0:T(8,128)(2,1)} %wk_ref.1, bf16[256,1024]{1,0:T(8,128)(2,1)} %wv_ref.1, bf16[256,256]{1,0:T(8,128)(2,1)} %wd_ref.1, bf16[2,128,1024]{2,1,0:T(8,128)(2,1)} %up_ref.1, f32[2,1024]{1,0:T(2,128)} %floor_ref.1, ...), custom_call_target="tpu_custom_call" | custom-call | tf_op jit(solution)/shard_map/halves/pallas_call | solution.py:926
  53.8 1.7 %copy.12 = bf16[1,128,1024]{2,1,0:T(8,128)(2,1)} copy(bf16[1,128,1024]{2,1,0:T(8,128)(2,1)} %bitcast.3) | data formatting | bytes 524288

commit v2 on v1

--- a/solution.py
+++ b/solution.py
@@ -46,6 +46,22 @@
     return x * mask
 
 
+WIDE = 128
+
+
+def lanes(x, p):
+    return x[:, p * WIDE : (p + 1) * WIDE]
+
+
+def by_head(x, y, mask, dims=None):
+    parts = []
+    for p in range(x.shape[1] // WIDE):
+        block = spread(lanes(y, p), mask)
+        a = lanes(x, p).astype(BF)
+        parts.append(mm(a, block) if dims is None else dot(a, block, dims))
+    return jnp.concatenate(parts, axis=1)
+
+
 def at_row(start, size):
     return pl.ds(pl.multiple_of(start, size), size)
 
@@ -54,7 +70,7 @@
     def __init__(self, tok, wk, wd, wv, wr, up, floor, rate, diag, gain, out, scratch):
         self.tok, self.wk, self.wd, self.wv, self.wr = tok, wk, wd, wv, wr
         self.up, self.floor, self.rate, self.diag, self.gain, self.out = up, floor, rate, diag, gain, out
-        (self.pk_s, self.pv_s, self.inv_s, self.grow_s, self.g_s, self.wp_s, self.kend_s,
+        (self.pk_s, self.pv_s, self.inv_s, self.grow_s, self.past_s, self.shrink_s, self.g_s, self.wp_s, self.kend_s,
          self.t_s, self.teg_s, self.step_s, self.tcv_s, self.put_s, self.state_s) = scratch
         self.length, self.chans = out.shape
         self.heads = self.chans // HEAD
@@ -65,52 +81,58 @@
     def unit(self, block):
         return at_row(block * SPAN, SPAN)
 
+    def decays(self, start):
+        chans, rank, tile = self.chans, self.rank, self.half
+        lowered = jnp.tanh(mm(self.tok[at_row(start, tile), :], self.wd[...])).astype(BF)
+        ri = iota((SPAN, SPAN), 0)
+        ci = iota((SPAN, SPAN), 1)
+        first = start // SPAN
+        pres = [
+            (mm(lowered[:, d * rank : (d + 1) * rank], self.up[d]) + self.floor[d : d + 1, :])
+            .astype(BF).astype(F32) for d in range(2)
+        ]
+        for s in range(tile // SPAN):
+            falls = [
+                -math.exp(-0.5) * jax.nn.sigmoid(pre[s * SPAN : (s + 1) * SPAN]) for pre in pres
+            ]
+            here = self.unit(first + s)
+            for d, fall in enumerate(falls):
+                tri = ((ci <= ri) if d == 0 else (ci >= ri)).astype(BF)
+                hi, lo = split(fall)
+                inside = mm(tri, hi) + mm(tri, lo)
+                mid = 0.5 * (inside[SPAN - 1 :] if d == 0 else inside[:1])
+                inside = inside - mid
+                self.grow_s[d, here, :] = jnp.exp(inside)
+                self.past_s[d, here, :] = jnp.exp(inside - fall)
+                self.shrink_s[d, here, :] = jnp.exp(-inside)
+                self.g_s[d, pl.ds(pl.multiple_of((first + s) * 8, 8), 8), :] = jnp.broadcast_to(
+                    jnp.exp(mid), (8, chans))
+
+    def g_of(self, d, block):
+        return self.g_s[d, pl.ds(pl.multiple_of(block * 8, 8), 8), :][:1]
+
     def keys(self, start):
-        chans, rank, tile = self.chans, self.rank, self.half
-        many = tile // SPAN
-        ones = head_ones(chans)
+        chans, tile = self.chans, self.half
         at = at_row(start, tile)
-        source = self.tok[at, :]
-        pk = mm(source, self.wk[...]).astype(BF)
+        first = start // SPAN
+        pk = mm(self.tok[at, :], self.wk[...]).astype(BF)
         self.pk_s[at, :] = pk
         pk = pk.astype(F32)
-        lowered = jnp.tanh(mm(source, self.wd[...])).astype(BF)
-        inv = lax.rsqrt(head_sum(pk * pk, ones) + 1.0)
+        inv = lax.rsqrt(head_sum(pk * pk, head_ones(chans)) + 1.0)
         self.inv_s[at, :] = inv
         normed = pk * inv
         rates = jax.nn.sigmoid(self.rate[...])
-        ri = iota((tile, tile), 0)
-        ci = iota((tile, tile), 1)
-        same = ri // SPAN == ci // SPAN
-        first = start // SPAN
         units = []
-        for d in range(2):
-            pre = (
-                mm(lowered[:, d * rank : (d + 1) * rank], self.up[d]) + self.floor[d : d + 1, :]
-            ).astype(BF).astype(F32)
-            fall = -math.exp(-0.5) * jax.nn.sigmoid(pre)
-            tri = jnp.logical_and(same, (ci <= ri) if d == 0 else (ci >= ri)).astype(BF)
-            hi, lo = split(fall)
-            inclusive = mm(tri, hi) + mm(tri, lo)
-            rated = normed * rates[d : d + 1, :]
-            for s in range(many):
-                cut = slice(s * SPAN, (s + 1) * SPAN)
-                inside = inclusive[cut]
-                end = inside[SPAN - 1 :] if d == 0 else inside[:1]
-                mid = 0.5 * end
-                inside = inside - mid
-                g = jnp.exp(mid)
-                grow = jnp.exp(inside)
-                e = -normed[cut] * jnp.exp(inside - fall[cut])
-                w = rated[cut] * jnp.exp(-inside)
-                here = self.unit(first + s)
-                self.grow_s[d, here, :] = grow
-                self.g_s[d, pl.ds(pl.multiple_of((first + s) * 8, 8), 8), :] = jnp.broadcast_to(g, (8, chans))
-                w = w.astype(BF)
-                kend = (w.astype(F32) * g).astype(BF)
-                self.wp_s[d, here, :] = w
-                self.kend_s[d, here, :] = kend
-                units.append((d, first + s, e.astype(BF), w, kend, (e * g).astype(BF)))
+        for s in range(tile // SPAN):
+            cut = slice(s * SPAN, (s + 1) * SPAN)
+            here = self.unit(first + s)
+            for d in range(2):
+                g = self.g_of(d, first + s)
+                e = -normed[cut] * self.past_s[d, here, :]
+                w = normed[cut] * rates[d : d + 1, :] * self.shrink_s[d, here, :]
+                self.wp_s[d, here, :] = w.astype(BF)
+                self.kend_s[d, here, :] = (w * g).astype(BF)
+                units.append((d, first + s, e.astype(BF), (e * g).astype(BF)))
         return units
 
     def strict(self, d):
@@ -120,48 +142,55 @@
 
     def invert(self, units):
         chans = self.chans
-        mask = head_ones(chans)
+        mask = head_ones(WIDE)
         ti = iota((SPAN, chans), 0)
         ji = iota((SPAN, chans), 1) % HEAD
         eye = (ti == ji).astype(F32)
         full = [
-            jnp.where(self.strict(d), dot(e, spread(w, mask), NT), 0.0) for d, _, e, w, _, _ in units
+            jnp.where(self.strict(d), by_head(e, self.wp_s[d, self.unit(block), :], mask, NT), 0.0)
+            for d, block, e, _ in units
         ]
         near = ti // 4 == ji // 4
         base = [jnp.where(near, a, 0.0) for a in full]
-        square = [mm(a.astype(BF), spread(a, mask)) for a in base]
+        square = [by_head(a, a, mask) for a in base]
         inverse = [eye + a for a in base]
-        inverse = [t + mm(t.astype(BF), spread(a2, mask)) for t, a2 in zip(inverse, square)]
+        inverse = [t + by_head(t, a2, mask) for t, a2 in zip(inverse, square)]
         size = 4
         while size < SPAN:
             far = jnp.logical_and(ti // (2 * size) == ji // (2 * size), ti // size != ji // size)
-            first = [
-                mm(t.astype(BF), spread(jnp.where(far, a, 0.0), mask))
-                for t, a in zip(inverse, full)
-            ]
-            inverse = [t + mm(f.astype(BF), spread(t, mask)) for t, f in zip(inverse, first)]
+            first = [by_head(t, jnp.where(far, a, 0.0), mask) for t, a in zip(inverse, full)]
+            inverse = [t + by_head(f, t, mask) for t, f in zip(inverse, first)]
             size *= 2
-        for (d, block, _, _, kend, eg), t in zip(units, inverse):
-            here = self.unit(block)
+        tegs = []
+        for (d, block, _, eg), t in zip(units, inverse):
             t = (t - eye).astype(BF)
-            self.t_s[d, here, :] = t
-            teg = (eg.astype(F32) + mm(t, spread(eg, mask))).astype(BF)
-            self.teg_s[d, here, :] = teg
-            self.step_s[d, at_row(block * chans, chans), :] = dot(teg, kend, TN).astype(BF) * mask
+            self.t_s[d, self.unit(block), :] = t
+            tegs.append((eg.astype(F32) + by_head(t, eg, mask)).astype(BF))
+        ones = head_ones(chans)
+        for (d, block, _, _), teg in zip(units, tegs):
+            self.teg_s[d, self.unit(block), :] = teg
+            self.step_s[d, at_row(block * chans, chans), :] = (
+                dot(teg, self.kend_s[d, self.unit(block), :], TN).astype(BF) * ones)
 
     def values(self):
         chans = self.chans
-        mask = head_ones(chans)
+        small = head_ones(WIDE)
+        mask = head_ones(chans).astype(F32)
         pv = mm(self.tok[...], self.wv[...]).astype(BF)
         self.pv_s[...] = pv
         cv = pv.astype(F32) / self.inv_s[...]
-        for block in range(self.blocks):
-            cut = slice(block * SPAN, (block + 1) * SPAN)
-            x = cv[cut]
-            for d in range(2):
-                tcv = x + mm(self.t_s[d, cut, :], spread(x, mask))
-                self.tcv_s[d, cut, :] = tcv
-                put = dot(tcv.astype(BF), self.kend_s[d, cut, :], TN) * mask.astype(F32)
+        each = 4
+        for group in range(0, self.blocks, each):
+            work = []
+            for block in range(group, min(group + each, self.blocks)):
+                cut = slice(block * SPAN, (block + 1) * SPAN)
+                for d in range(2):
+                    tcv = cv[cut] + by_head(self.t_s[d, cut, :], cv[cut], small)
+                    self.tcv_s[d, cut, :] = tcv
+                    work.append((d, cut, tcv.astype(BF)))
+            puts = [dot(tcv, self.kend_s[d, cut, :], TN) for d, cut, tcv in work]
+            for (d, cut, _), put in zip(work, puts):
+                put = put * mask
                 self.put_s[d, cut, :] = sum(put[h * HEAD : (h + 1) * HEAD] for h in range(self.heads))
 
     def scan(self):
@@ -178,39 +207,42 @@
                     step_w = self.step_s[d, block * self.chans : (block + 1) * self.chans, :]
                     states[d] = state * (g * g) + mm(low, step_w) + self.put_s[d, cut, :]
 
-    def outputs(self, start, tile):
-        chans = self.chans
-        mask = head_ones(chans)
+    def outputs(self, start, tile, p):
+        mask = head_ones(WIDE)
         at = at_row(start, tile)
+        cols = slice(p * WIDE, (p + 1) * WIDE)
         first = start // SPAN
-        pr = mm(self.tok[at, :], self.wr[...]).astype(BF).astype(F32)
-        pp = pr * self.pk_s[at, :].astype(F32)
-        rates = jax.nn.sigmoid(self.rate[...])
-        both = jnp.sum(rates * self.diag[...], axis=0, keepdims=True)
-        total = head_sum(pp * both, mask) * self.pv_s[at, :].astype(F32)
-        inv = self.inv_s[at, :]
-        for d in range(2):
-            ys = []
-            diag = head_sum(pp * rates[d : d + 1, :], mask) * inv
-            for s in range(tile // SPAN):
-                cut = slice(s * SPAN, (s + 1) * SPAN)
-                here = self.unit(first + s)
-                g = self.g_s[d, pl.ds(pl.multiple_of((first + s) * 8, 8), 8), :][:1]
-                q = pr[cut] * self.grow_s[d, here, :]
-                qb = q.astype(BF)
-                qg = (q * g).astype(BF)
-                b = jnp.where(self.strict(d), dot(qb, spread(self.wp_s[d, here, :], mask), NT), 0.0)
-                read = dot(
-                    jnp.concatenate([self.teg_s[d, here, :], qg], axis=0),
-                    spread(self.state_s[d, here, :], mask), NT,
-                )
-                exact = self.tcv_s[d, here, :] + read[:SPAN]
-                ys.append(read[SPAN:] + mm(b.astype(BF), spread(exact, mask)) + diag[cut] * exact)
-            y = jnp.concatenate(ys, axis=0)
-            centred = y - head_sum(y, mask) * (1.0 / HEAD)
-            variance = head_sum(centred * centred, mask) * (1.0 / HEAD)
-            total = total + centred * lax.rsqrt(variance + 0.00064) * self.gain[...]
-        self.out[at, :] = total.astype(BF)
+        pr = mm(self.tok[at, :], self.wr[:, cols]).astype(BF).astype(F32)
+        pp = pr * self.pk_s[at, cols].astype(F32)
+        rates = jax.nn.sigmoid(self.rate[:, cols])
+        both = jnp.sum(rates * self.diag[:, cols], axis=0, keepdims=True)
+        inv = self.inv_s[at, cols]
+        total = head_sum(pp * both, mask) * self.pv_s[at, cols].astype(F32)
+        diags = [head_sum(pp * rates[d : d + 1, :], mask) * inv for d in range(2)]
+        ti = iota((SPAN, WIDE), 0)
+        ji = iota((SPAN, WIDE), 1) % HEAD
+        units = [(d, s) for s in range(tile // SPAN) for d in range(2)]
+        bs, reads = [], []
+        for d, s in units:
+            here = self.unit(first + s)
+            q = pr[s * SPAN : (s + 1) * SPAN] * self.grow_s[d, here, cols]
+            bs.append(by_head(q, self.wp_s[d, here, cols], mask, NT))
+            g = self.g_s[d, pl.ds(pl.multiple_of((first + s) * 8, 8), 8), cols][:1]
+            lhs = jnp.concatenate([self.teg_s[d, here, cols], (q * g).astype(BF)], axis=0)
+            reads.append(by_head(lhs, self.state_s[d, here, cols], mask, NT))
+        ys = [[], []]
+        for (d, s), b, read in zip(units, bs, reads):
+            exact = self.tcv_s[d, self.unit(first + s), cols] + read[:SPAN]
+            b = jnp.where((ti > ji) if d == 0 else (ti < ji), b, 0.0)
+            ys[d].append(
+                read[SPAN:] + by_head(b, exact, mask) + diags[d][s * SPAN : (s + 1) * SPAN] * exact)
+        ys = [jnp.concatenate(y, axis=0) for y in ys]
+        means = [head_sum(y, mask) * (1.0 / HEAD) for y in ys]
+        centred = [y - mean for y, mean in zip(ys, means)]
+        variances = [head_sum(c * c, mask) * (1.0 / HEAD) for c in centred]
+        for c, variance in zip(centred, variances):
+            total = total + c * lax.rsqrt(variance + 0.00064) * self.gain[:, cols]
+        self.out[at, cols] = total.astype(BF)
 
 
 def core_scratch(length, chans):
@@ -219,7 +251,8 @@
     blocks = length // SPAN
     return [
         vm((length, chans), BF), vm((length, chans), BF), vm((length, chans), F32),
-        both(length, F32), both(blocks * 8, F32), both(length, BF), both(length, BF),
+        both(length, F32), both(length, F32), both(length, F32), both(blocks * 8, F32),
+        both(length, BF), both(length, BF),
         both(length, BF), both(length, BF), both(blocks * chans, BF), both(length, F32),
         both(length, F32), both(length, BF),
     ]
@@ -605,60 +638,71 @@
         return copy
 
     sent = []
-    pieces = [(wk_ref, wk_all), (wv_ref, wv_all), (wr_ref, wr_all)]
+    wide = chans // WIDE
+    pieces = [(wk_ref, wk_all, 0, chans), (wv_ref, wv_all, 0, chans)]
+    pieces += [(wr_ref, wr_all, p * WIDE, WIDE) for p in range(wide)]
+    decay = len(pieces)
+
+    def take(n, who):
+        src, _, low, size = pieces[n]
+        return src.at[:, pl.ds(pl.multiple_of(who * chans + low, WIDE), size)]
+
+    def landing(n, block):
+        _, dst, low, size = pieces[n]
+        return dst.at[block, low : low + size]
 
     def direct(n):
-        src, dst = pieces[n]
         for i, p in enumerate(x_peers + y_peers):
             for k in range(2):
                 sent.append(go(remote(
-                    src.at[:, cols(u * 2 + k)], dst.at[mine, :],
+                    take(n, u * 2 + k), landing(n, mine),
                     w_out.at[n, i * 2 + k], w_in.at[n, me], (z, p * 2 + k),
                 )))
         last = 2 * len(x_peers + y_peers)
         sent.append(go(remote(
-            src.at[:, cols(u * 2 + 1 - core)], dst.at[mine, :],
+            take(n, u * 2 + 1 - core), landing(n, mine),
             w_out.at[n, last], w_in.at[n, me], (z, partner),
         )))
 
+    def wait_for(sem, dst):
+        remote(dst, dst, sem, sem, (z, partner)).wait_recv()
+
     def arrived(sem, dst, block):
-        remote(dst.at[block, :], dst.at[block, :], sem, sem, (z, partner)).wait_recv()
+        wait_for(sem, dst.at[block, :])
 
     def w_rows(p, c):
         return at_row((p * 2 + c) * depth, depth)
 
     def relay(n):
-        dst = pieces[n][1]
         count = 0
         for c, froms, tos in ((0, x_peers, y_peers), (1, y_peers, x_peers)):
             for p in froms:
                 block = w_rows(p, c)
-                arrived(w_in.at[n, p * 2 + c], dst, block)
+                wait_for(w_in.at[n, p * 2 + c], landing(n, block))
                 for q in tos:
                     sent.append(go(remote(
-                        dst.at[block, :], dst.at[block, :],
+                        landing(n, block), landing(n, block),
                         relay_out.at[n, count], w_in.at[n, p * 2 + c], (z, q * 2 + core),
                     )))
                     count += 1
 
     def finish(n):
-        dst = pieces[n][1]
         for c, others in ((1, x_peers), (0, y_peers)):
             for p in others:
-                arrived(w_in.at[n, p * 2 + c], dst, w_rows(p, c))
+                wait_for(w_in.at[n, p * 2 + c], landing(n, w_rows(p, c)))
         for ky in range(1, other):
             for kx in range(1, side):
                 p = lax.rem(cy + ky, other) * side + lax.rem(cx + kx, side)
                 for c in range(2):
-                    arrived(w_in.at[n, p * 2 + c], dst, w_rows(p, c))
-        arrived(w_in.at[n, partner], dst, w_rows(chip, 1 - core))
+                    wait_for(w_in.at[n, p * 2 + c], landing(n, w_rows(p, c)))
+        wait_for(w_in.at[n, partner], landing(n, w_rows(chip, 1 - core)))
 
     def decay_direct():
         for i, p in enumerate(x_peers + y_peers):
             sent.append(go(remote(
-                wd_ref, wd_all.at[mine, :], w_out.at[3, i], d_in.at[me], (z, p * 2 + core))))
+                wd_ref, wd_all.at[mine, :], w_out.at[decay, i], d_in.at[me], (z, p * 2 + core))))
         sent.append(go(remote(
-            wd_ref, wd_all.at[mine, :], w_out.at[3, len(x_peers + y_peers)], d_in.at[me], (z, partner))))
+            wd_ref, wd_all.at[mine, :], w_out.at[decay, len(x_peers + y_peers)], d_in.at[me], (z, partner))))
 
     def decay_pass(p, n):
         block = w_rows(p, core)
@@ -678,7 +722,7 @@
                     for q in tos:
                         go(remote(
                             wd_all.at[block, :], wd_all.at[block, :],
-                            relay_out.at[3, count], d_in.at[p * 2 + c], (z, q * 2 + c)))
+                            relay_out.at[decay, count], d_in.at[p * 2 + c], (z, q * 2 + c)))
                         count += 1
                 for p in tos:
                     arrived(d_in.at[p * 2 + c], wd_all, w_rows(p, c))
@@ -692,7 +736,7 @@
                         for q in tos:
                             remote(
                                 wd_all.at[block, :], wd_all.at[block, :],
-                                relay_out.at[3, count], d_in.at[p * 2 + c], (z, q * 2 + c)).wait_send()
+                                relay_out.at[decay, count], d_in.at[p * 2 + c], (z, q * 2 + c)).wait_send()
                             count += 1
 
             late.append(close)
@@ -802,12 +846,18 @@
     for n in range(len(sources)):
         take_tokens(n)
     decay_finish()
-    finish(0)
-    for copy in own[:4]:
-        copy.wait()
+    for n in (0, 2, 3):
+        own[n].wait()
     own_tokens()
     for n in range(half - 1):
         passed_tokens(n)
+    work = Core(
+        tok_all, wk_all, wd_all, wv_all, wr_all, up_s, floor_s, rate_s, diag_s, gain_s, out_all, scratch)
+    near_rows = h * half * rows
+    far_rows = (1 - h) * half * rows
+    work.decays(near_rows)
+    finish(0)
+    own[1].wait()
 
     @pl.when(jnp.logical_not(stay))
     def _():
@@ -816,41 +866,51 @@
     for n, (src, dst) in enumerate(smalls):
         remote(dst, dst, p_in.at[n], p_in.at[n], (z, partner)).wait_recv()
 
-    work = Core(
-        tok_all, wk_all, wd_all, wv_all, wr_all, up_s, floor_s, rate_s, diag_s, gain_s, out_all, scratch)
-    near_rows = h * half * rows
-    far_rows = (1 - h) * half * rows
     units = work.keys(near_rows)
-    relay(1)
     work.invert(units)
     for n in range(half - 1, len(sources)):
         passed_tokens(n)
+    work.decays(far_rows)
     units = work.keys(far_rows)
+    relay(1)
+    for p in range(1, wide):
+        direct(2 + p)
+    work.invert(units)
     relay(2)
-    work.invert(units)
     finish(1)
     own[4].wait()
     work.values()
     work.scan()
-    finish(2)
+
+    def give(s, p, n, act):
+        block = at_row(s * rows, rows)
+        low = p * WIDE
+        act(remote(
+            out_all.at[block, low : low + WIDE],
+            out_ref.at[:, pl.ds(pl.multiple_of(slot * chans + low, WIDE), WIDE)],
+            o_out.at[p, n], o_in.at[p, slot], (s, chip * 2 + h)))
+
+    def give_far(p, act):
+        for v in range(half):
+            give(layer(1 - h, v), p, v, act)
+
+    def give_near(p, act):
+        for n in range(half - 1):
+            give(sources[n][0], p, half + n, act)
+
+        @pl.when(core != h)
+        def _():
+            give(z, p, sp - 1, act)
+
     own[5].wait()
-
-    def give(s, n, act):
-        block = at_row(s * rows, rows)
-        act(remote(
-            out_all.at[block, :], out_ref.at[:, cols(slot)], o_out.at[n], o_in.at[slot],
-            (s, chip * 2 + h)))
-
-    work.outputs(far_rows, half * rows)
-    for v in range(half):
-        give(layer(1 - h, v), v, go)
-    work.outputs(near_rows, half * rows)
-    for n in range(half - 1):
-        give(sources[n][0], half + n, go)
-
-    @pl.when(core != h)
-    def _():
-        give(z, sp - 1, go)
+    for p in range(wide):
+        if p + 1 < wide:
+            relay(3 + p)
+        finish(2 + p)
+        work.outputs(far_rows, half * rows, p)
+        give_far(p, go)
+        work.outputs(near_rows, half * rows, p)
+        give_near(p, go)
 
     @pl.when(core == h)
     def _():
@@ -866,21 +926,15 @@
         copy.wait_send()
     for close in late:
         close()
-    for v in range(half):
-        give(layer(1 - h, v), v, stop)
-    for n in range(half - 1):
-        give(sources[n][0], half + n, stop)
-
-    @pl.when(core != h)
-    def _():
-        give(z, sp - 1, stop)
-
-    for g in range(sp):
-        @pl.when(jnp.logical_not(jnp.logical_and(core == h, slot == g)))
-        def _():
-            remote(
-                out_all.at[pl.ds(0, rows), :], out_ref.at[:, g * chans : (g + 1) * chans],
-                o_in.at[g], o_in.at[g], (z, partner)).wait_recv()
+    for p in range(wide):
+        give_far(p, stop)
+        give_near(p, stop)
+        for g in range(sp):
+            low = g * chans + p * WIDE
+
+            @pl.when(jnp.logical_not(jnp.logical_and(core == h, slot == g)))
+            def _():
+                wait_for(o_in.at[p, g], out_ref.at[:, low : low + WIDE])
 
 
 def halves_call(sp, dp, side, rows, width, depth, chans, rank):
@@ -891,6 +945,7 @@
     peers = side + other - 2
     corners = (side - 1) * (other - 1)
     length = rows * sp
+    wide = chans // WIDE
     return pl.pallas_call(
         functools.partial(halves_kernel, sp, side, other),
         out_shape=jax.ShapeDtypeStruct((rows, chans * sp), BF),
@@ -900,8 +955,8 @@
             vm((length, width), BF), vm((width, chans), BF), vm((width, chans), BF), vm((width, chans), BF),
             vm((width, 2 * rank), BF), vm((2, rank, chans), BF), vm((2, chans), F32), vm((2, chans), F32),
             vm((2, chans), F32), vm((1, chans), F32), vm((length, chans), BF),
-            dma((3, dp)), dma((4, 2 * peers + 1)), dma((4, 2 * corners)), dma((dp,)), dma((peers + corners,)),
-            dma((sp,)), dma((sp,)), dma((5,)), dma((2 * sp,)), dma((3,)), dma((3,)), dma((sp,)), dma((sp,)),
+            dma((2 + wide, dp)), dma((3 + wide, 2 * peers + 1)), dma((3 + wide, 2 * corners)), dma((dp,)), dma((peers + corners,)),
+            dma((sp,)), dma((sp,)), dma((5,)), dma((2 * sp,)), dma((3,)), dma((3,)), dma((wide, sp)), dma((wide, sp)),
             dma((7,)),
         ] + core_scratch(length, chans),
         compiler_params=pltpu.CompilerParams(

time: 55.6 us -> 56.4 us (1.014)
  Pallas kernels: 53.8 us -> 54.6 us
    pallas_call x1, Pallas kernels: 53.8 us -> 54.6 us  [per_device(): halves_call(sp, dp, side, rows, width, depth, chans, decay_up_weight.shap...]
where the time goes in v2:
time: 56.4 us; the launch traced here: 56.2 us
  Pallas kernels  54.6 us (97%)
  local copies, waits for them, and re-layouts  1.67 us (3%)
    pallas_call x1, Pallas kernels, per_device(): halves_call(sp, dp, side, rows, width, depth, chans, decay_up_weight.shap...  54.6 us
    unnamed x1, local copies, waits for them, and re-layouts  1.67 us

profile of v2, /device:TPU:0, one launch (start us, length us, event | category | flops | bytes accessed | tf_op | source)
XLA Modules:
  0.0 56.2 jit_solution(14443567611691361706)
XLA Ops:
  0.0 54.6 %halves.1 = bf16[128,1024]{1,0:T(8,128)(2,1)} custom-call(bf16[128,2048]{1,0:T(8,128)(2,1)} %bitcast.4, bf16[256,1024]{1,0:T(8,128)(2,1)} %wr_ref.1, bf16[256,1024]{1,0:T(8,128)(2,1)} %wk_ref.1, bf16[256,1024]{1,0:T(8,128)(2,1)} %wv_ref.1, bf16[256,256]{1,0:T(8,128)(2,1)} %wd_ref.1, bf16[2,128,1024]{2,1,0:T(8,128)(2,1)} %up_ref.1, f32[2,1024]{1,0:T(2,128)} %floor_ref.1, ...), custom_call_target="tpu_custom_call" | custom-call | tf_op jit(solution)/shard_map/halves/pallas_call | solution.py:981
  54.6 1.7 %copy.12 = bf16[1,128,1024]{2,1,0:T(8,128)(2,1)} copy(bf16[1,128,1024]{2,1,0:T(8,128)(2,1)} %bitcast.3) | data formatting | bytes 524288

commit v3 on v2

--- a/solution.py
+++ b/solution.py
@@ -35,7 +35,9 @@
 
 def head_sum(x, ones):
     hi, lo = split(x)
-    return mm(hi, ones) + mm(lo, ones)
+    if ones.shape[0] > WIDE:
+        return mm(hi, ones) + mm(lo, ones)
+    return mm(jnp.concatenate([hi, lo], axis=1), jnp.concatenate([ones, ones], axis=0))
 
 
 def spread(x, mask):
@@ -573,7 +575,7 @@
     depth = wk_ref.shape[0]
     chans = wk_all.shape[1]
     half = sp // 2
-    part = rows // 2
+    part = rows // 4
     z = lax.axis_index("sp")
     me = lax.axis_index("dp")
     core = me % 2
@@ -761,40 +763,40 @@
         return at_row(s * rows + i * part, part)
 
     def block_sends(act):
-        def both_parts(target_layer, first):
-            for i in range(2):
+        def all_parts(target_layer, first):
+            for i in range(4):
                 act(remote(
                     tok_ref.at[pl.ds(i * part, part), :], tok_all.at[t_rows(z, i), :],
-                    t_out.at[first + i], t_in.at[z], (target_layer, chip * 2 + i)))
+                    t_out.at[first + i], t_in.at[z, i // 2], (target_layer, chip * 2 + i % 2)))
 
         @pl.when(core != h)
         def _():
-            both_parts(layer(core, 0), 0)
+            all_parts(layer(core, 0), 0)
 
         @pl.when(jnp.logical_and(core == h, u + 1 < half))
         def _():
-            both_parts(layer(h, u + 1), 0)
+            all_parts(layer(h, u + 1), 0)
 
         @pl.when(jnp.logical_and(core == h, u > 0))
         def _():
-            both_parts(layer(h, u - 1), 2)
+            all_parts(layer(h, u - 1), 4)
 
         @pl.when(core == h)
         def _():
             act(remote(
-                tok_ref, tok_all.at[at_row(z * rows, rows), :], t_out.at[4], t_pass.at[z], (z, partner)))
-
-    def forward(s, outward, inward, n, act):
-        block = t_rows(s, core)
+                tok_ref, tok_all.at[at_row(z * rows, rows), :], t_out.at[8], t_pass.at[z, 0], (z, partner)))
+
+    def forward(s, outward, inward, n, q, act):
+        block = t_rows(s, 2 * q + core)
         for cond, step in ((outward, 1), (inward, -1)):
             if cond is not None:
                 @pl.when(cond)
                 def _():
                     act(remote(
-                        tok_all.at[block, :], tok_all.at[block, :], t_fwd.at[n], t_in.at[s],
+                        tok_all.at[block, :], tok_all.at[block, :], t_fwd.at[0, n, q], t_in.at[s, q],
                         (layer(h, u + step), me)))
         act(remote(
-            tok_all.at[block, :], tok_all.at[block, :], t_fwd.at[sp + n], t_pass.at[s], (z, partner)))
+            tok_all.at[block, :], tok_all.at[block, :], t_fwd.at[1, n, q], t_pass.at[s, q], (z, partner)))
 
     near = [lax.rem(u + k, half) for k in range(1, half)]
     sources = [
@@ -802,10 +804,16 @@
     ]
     sources += [(layer(1 - h, v), u + 1 < half, None) for v in range(half)]
 
-    def take_tokens(n):
+    def take_tokens(n, q):
         s, outward, inward = sources[n]
-        arrived(t_in.at[s], tok_all, t_rows(s, core))
-        forward(s, outward, inward, n, go)
+        arrived(t_in.at[s, q], tok_all, t_rows(s, 2 * q + core))
+        forward(s, outward, inward, n, q, go)
+
+    def take_far(now, q):
+        @pl.when(now)
+        def _():
+            for n in range(half - 1, len(sources)):
+                take_tokens(n, q)
 
     def own_tokens():
         block = at_row(z * rows, rows)
@@ -816,11 +824,12 @@
 
         @pl.when(core != h)
         def _():
-            arrived(t_pass.at[z], tok_all, block)
+            arrived(t_pass.at[z, 0], tok_all, block)
 
     def passed_tokens(n):
         s = sources[n][0]
-        arrived(t_pass.at[s], tok_all, t_rows(s, 1 - core))
+        for q in range(2):
+            arrived(t_pass.at[s, q], tok_all, t_rows(s, 2 * q + 1 - core))
 
     goal = (layer(core, z // 2), chip * 2 + z % 2)
     stay = jnp.logical_and(goal[0] == z, z % 2 == core)
@@ -840,11 +849,14 @@
     block_sends(go)
     direct(0)
     decay_relay()
+    take_far(u + 1 < half, 0)
     relay(0)
     direct(1)
     direct(2)
-    for n in range(len(sources)):
-        take_tokens(n)
+    for n in range(half - 1):
+        for q in range(2):
+            take_tokens(n, q)
+    take_far(u + 1 < half, 1)
     decay_finish()
     for n in (0, 2, 3):
         own[n].wait()
@@ -856,6 +868,7 @@
     near_rows = h * half * rows
     far_rows = (1 - h) * half * rows
     work.decays(near_rows)
+    take_far(u + 1 == half, 0)
     finish(0)
     own[1].wait()
 
@@ -868,6 +881,7 @@
 
     units = work.keys(near_rows)
     work.invert(units)
+    take_far(u + 1 == half, 1)
     for n in range(half - 1, len(sources)):
         passed_tokens(n)
     work.decays(far_rows)
@@ -921,7 +935,8 @@
 
     block_sends(stop)
     for n, (s, outward, inward) in enumerate(sources):
-        forward(s, outward, inward, n, stop)
+        for q in range(2):
+            forward(s, outward, inward, n, q, stop)
     for copy in sent:
         copy.wait_send()
     for close in late:
@@ -956,7 +971,7 @@
             vm((width, 2 * rank), BF), vm((2, rank, chans), BF), vm((2, chans), F32), vm((2, chans), F32),
             vm((2, chans), F32), vm((1, chans), F32), vm((length, chans), BF),
             dma((2 + wide, dp)), dma((3 + wide, 2 * peers + 1)), dma((3 + wide, 2 * corners)), dma((dp,)), dma((peers + corners,)),
-            dma((sp,)), dma((sp,)), dma((5,)), dma((2 * sp,)), dma((3,)), dma((3,)), dma((wide, sp)), dma((wide, sp)),
+            dma((sp, 2)), dma((sp, 2)), dma((9,)), dma((2, sp, 2)), dma((3,)), dma((3,)), dma((wide, sp)), dma((wide, sp)),
             dma((7,)),
         ] + core_scratch(length, chans),
         compiler_params=pltpu.CompilerParams(
@@ -977,7 +992,7 @@
     chans = channels // sp
     side = math.isqrt(dp // 2)
     gain = head_norm_gain[None, :]
-    if chans % 128 == 0 and sp % 2 == 0 and dp == 2 * side * side and rows % (2 * SPAN) == 0:
+    if chans % 128 == 0 and sp % 2 == 0 and dp == 2 * side * side and rows % SPAN == 0:
         mixed = halves_call(sp, dp, side, rows, width, depth, chans, decay_up_weight.shape[1])(
             tokens[0], receptance_weight, key_projection_weight, value_projection_weight, decay_down_weight,
             decay_up_weight, decay_floor_level, correction_rate_logit, diagonal_address_factor, gain)

time: 56.4 us -> 49.4 us (0.88)
  Pallas kernels: 54.6 us -> 47.5 us
    pallas_call x1, Pallas kernels: 54.6 us -> 47.5 us  [per_device(): halves_call(sp, dp, side, rows, width, depth, chans, decay_up_weight.shap...]
where the time goes in v3:
time: 49.4 us; the launch traced here: 49.2 us
  Pallas kernels  47.5 us (96%)
  local copies, waits for them, and re-layouts  1.67 us (3%)
    pallas_call x1, Pallas kernels, per_device(): halves_call(sp, dp, side, rows, width, depth, chans, decay_up_weight.shap...  47.5 us
    unnamed x1, local copies, waits for them, and re-layouts  1.67 us

profile of v3, /device:TPU:0, one launch (start us, length us, event | category | flops | bytes accessed | tf_op | source)
XLA Modules:
  0.0 49.2 jit_solution(17204589970866686690)
XLA Ops:
  0.0 47.5 %halves.1 = bf16[128,1024]{1,0:T(8,128)(2,1)} custom-call(bf16[128,2048]{1,0:T(8,128)(2,1)} %bitcast.4, bf16[256,1024]{1,0:T(8,128)(2,1)} %wr_ref.1, bf16[256,1024]{1,0:T(8,128)(2,1)} %wk_ref.1, bf16[256,1024]{1,0:T(8,128)(2,1)} %wv_ref.1, bf16[256,256]{1,0:T(8,128)(2,1)} %wd_ref.1, bf16[2,128,1024]{2,1,0:T(8,128)(2,1)} %up_ref.1, f32[2,1024]{1,0:T(2,128)} %floor_ref.1, ...), custom_call_target="tpu_custom_call" | custom-call | tf_op jit(solution)/shard_map/halves/pallas_call | solution.py:996
  47.5 1.7 %copy.12 = bf16[1,128,1024]{2,1,0:T(8,128)(2,1)} copy(bf16[1,128,1024]{2,1,0:T(8,128)(2,1)} %bitcast.3) | data formatting | bytes 524288

commit v4 on v3

--- a/solution.py
+++ b/solution.py
@@ -882,18 +882,20 @@
     units = work.keys(near_rows)
     work.invert(units)
     take_far(u + 1 == half, 1)
+    relay(1)
+    for p in range(1, wide):
+        direct(2 + p)
     for n in range(half - 1, len(sources)):
         passed_tokens(n)
     work.decays(far_rows)
     units = work.keys(far_rows)
-    relay(1)
-    for p in range(1, wide):
-        direct(2 + p)
     work.invert(units)
     relay(2)
     finish(1)
     own[4].wait()
     work.values()
+    for p in range(1, wide):
+        relay(2 + p)
     work.scan()
 
     def give(s, p, n, act):
@@ -918,8 +920,6 @@
 
     own[5].wait()
     for p in range(wide):
-        if p + 1 < wide:
-            relay(3 + p)
         finish(2 + p)
         work.outputs(far_rows, half * rows, p)
         give_far(p, go)
@@ -975,7 +975,7 @@
             dma((7,)),
         ] + core_scratch(length, chans),
         compiler_params=pltpu.CompilerParams(
-            vmem_limit_bytes=58 * 1024 * 1024, collective_id=0, has_side_effects=True
+            vmem_limit_bytes=32 * 1024 * 1024, collective_id=0, has_side_effects=True
         ),
         name="halves",
     )
@@ -993,9 +993,11 @@
     side = math.isqrt(dp // 2)
     gain = head_norm_gain[None, :]
     if chans % 128 == 0 and sp % 2 == 0 and dp == 2 * side * side and rows % SPAN == 0:
-        mixed = halves_call(sp, dp, side, rows, width, depth, chans, decay_up_weight.shape[1])(
+        given = [
             tokens[0], receptance_weight, key_projection_weight, value_projection_weight, decay_down_weight,
-            decay_up_weight, decay_floor_level, correction_rate_logit, diagonal_address_factor, gain)
+            decay_up_weight, decay_floor_level, correction_rate_logit, diagonal_address_factor, gain]
+        given = [pltpu.with_memory_space_constraint(x, pltpu.HBM) for x in given]
+        mixed = halves_call(sp, dp, side, rows, width, depth, chans, decay_up_weight.shape[1])(*given)
         return mixed[None]
     start = lax.axis_index("sp") * chans
 

time: 49.4 us -> 47 us (0.951)
  Pallas kernels: 47.5 us -> 46.1 us
  local copies, waits for them, and re-layouts: 1.67 us -> 0.71 us
    pallas_call x1, Pallas kernels: 47.5 us -> 46.1 us  [per_device(): halves_call(sp, dp, side, rows, width, depth, chans, decay_up_weight.shap...]
    unnamed x1, local copies, waits for them, and re-layouts: 1.67 us -> 0.71 us
where the time goes in v4:
time: 47 us; the launch traced here: 46.8 us
  Pallas kernels  46.1 us (98%)
  local copies, waits for them, and re-layouts  0.71 us (2%)
    pallas_call x1, Pallas kernels, per_device(): halves_call(sp, dp, side, rows, width, depth, chans, decay_up_weight.shap...  46.1 us

profile of v4, /device:TPU:0, one launch (start us, length us, event | category | flops | bytes accessed | tf_op | source)
XLA Modules:
  0.0 46.8 jit_solution(2581792040469740416)
XLA Ops:
  0.0 46.1 %halves.1 = bf16[128,1024]{1,0:T(8,128)(2,1)S(1)} custom-call(bf16[128,2048]{1,0:T(8,128)(2,1)} %bitcast.4, bf16[256,1024]{1,0:T(8,128)(2,1)} %wr_ref.1, bf16[256,1024]{1,0:T(8,128)(2,1)} %wk_ref.1, bf16[256,1024]{1,0:T(8,128)(2,1)} %wv_ref.1, bf16[256,256]{1,0:T(8,128)(2,1)} %wd_ref.1, bf16[2,128,1024]{2,1,0:T(8,128)(2,1)} %up_ref.1, f32[2,1024]{1,0:T(2,128)} %floor_ref.1, ...), custom_call_target="tpu_custom_call" | custom-call | tf_op jit(solution)/shard_map/halves/pallas_call | solution.py:1000
  46.1 0.7 %copy.12 = bf16[1,128,1024]{2,1,0:T(8,128)(2,1)} copy(bf16[1,128,1024]{2,1,0:T(8,128)(2,1)S(1)} %bitcast.3) | data formatting | bytes 524288

commit v5 on v4

--- a/solution.py
+++ b/solution.py
@@ -68,6 +68,11 @@
     return pl.ds(pl.multiple_of(start, size), size)
 
 
+def halved(tok, start, size, w):
+    part = size // 2
+    return jnp.concatenate([mm(tok[at_row(start + i * part, part), :], w) for i in range(2)], axis=0)
+
+
 class Core:
     def __init__(self, tok, wk, wd, wv, wr, up, floor, rate, diag, gain, out, scratch):
         self.tok, self.wk, self.wd, self.wv, self.wr = tok, wk, wd, wv, wr
@@ -85,7 +90,7 @@
 
     def decays(self, start):
         chans, rank, tile = self.chans, self.rank, self.half
-        lowered = jnp.tanh(mm(self.tok[at_row(start, tile), :], self.wd[...])).astype(BF)
+        lowered = jnp.tanh(halved(self.tok, start, tile, self.wd[...])).astype(BF)
         ri = iota((SPAN, SPAN), 0)
         ci = iota((SPAN, SPAN), 1)
         first = start // SPAN
@@ -117,7 +122,7 @@
         chans, tile = self.chans, self.half
         at = at_row(start, tile)
         first = start // SPAN
-        pk = mm(self.tok[at, :], self.wk[...]).astype(BF)
+        pk = halved(self.tok, start, tile, self.wk[...]).astype(BF)
         self.pk_s[at, :] = pk
         pk = pk.astype(F32)
         inv = lax.rsqrt(head_sum(pk * pk, head_ones(chans)) + 1.0)
@@ -178,9 +183,9 @@
         chans = self.chans
         small = head_ones(WIDE)
         mask = head_ones(chans).astype(F32)
-        pv = mm(self.tok[...], self.wv[...]).astype(BF)
-        self.pv_s[...] = pv
-        cv = pv.astype(F32) / self.inv_s[...]
+        for r in range(0, self.length, self.half):
+            self.pv_s[r : r + self.half, :] = mm(self.tok[r : r + self.half, :], self.wv[...]).astype(BF)
+        cv = self.pv_s[...].astype(F32) / self.inv_s[...]
         each = 4
         for group in range(0, self.blocks, each):
             work = []
@@ -882,12 +887,12 @@
     units = work.keys(near_rows)
     work.invert(units)
     take_far(u + 1 == half, 1)
+    for n in range(half - 1, len(sources)):
+        passed_tokens(n)
+    work.decays(far_rows)
     relay(1)
     for p in range(1, wide):
         direct(2 + p)
-    for n in range(half - 1, len(sources)):
-        passed_tokens(n)
-    work.decays(far_rows)
     units = work.keys(far_rows)
     work.invert(units)
     relay(2)
@@ -907,7 +912,7 @@
             o_out.at[p, n], o_in.at[p, slot], (s, chip * 2 + h)))
 
     def give_far(p, act):
-        for v in range(half):
+        for v in reversed(range(half)):
             give(layer(1 - h, v), p, v, act)
 
     def give_near(p, act):

time: 47 us -> 46.4 us (0.987)
  Pallas kernels: 46.1 us -> 45.5 us
    pallas_call x1, Pallas kernels: 46.1 us -> 45.5 us  [per_device(): halves_call(sp, dp, side, rows, width, depth, chans, decay_up_weight.shap...]
where the time goes in v5:
time: 46.4 us; the launch traced here: 46.2 us
  Pallas kernels  45.5 us (98%)
  local copies, waits for them, and re-layouts  0.71 us (2%)
    pallas_call x1, Pallas kernels, per_device(): halves_call(sp, dp, side, rows, width, depth, chans, decay_up_weight.shap...  45.5 us

profile of v5, /device:TPU:0, one launch (start us, length us, event | category | flops | bytes accessed | tf_op | source)
XLA Modules:
  0.0 46.2 jit_solution(6950610267609191807)
XLA Ops:
  0.0 45.5 %halves.1 = bf16[128,1024]{1,0:T(8,128)(2,1)S(1)} custom-call(bf16[128,2048]{1,0:T(8,128)(2,1)} %bitcast.4, bf16[256,1024]{1,0:T(8,128)(2,1)} %wr_ref.1, bf16[256,1024]{1,0:T(8,128)(2,1)} %wk_ref.1, bf16[256,1024]{1,0:T(8,128)(2,1)} %wv_ref.1, bf16[256,256]{1,0:T(8,128)(2,1)} %wd_ref.1, bf16[2,128,1024]{2,1,0:T(8,128)(2,1)} %up_ref.1, f32[2,1024]{1,0:T(2,128)} %floor_ref.1, ...), custom_call_target="tpu_custom_call" | custom-call | tf_op jit(solution)/shard_map/halves/pallas_call | solution.py:1005
  45.5 0.7 %copy.12 = bf16[1,128,1024]{2,1,0:T(8,128)(2,1)} copy(bf16[1,128,1024]{2,1,0:T(8,128)(2,1)S(1)} %bitcast.3) | data formatting | bytes 524288
